TPU v7x, 32 devices: a whole 2x2x4 slice. The times are simulated.
32 devices in a mesh: sp: 8 (over z, y), tp: 4 (over x, core).
Axes of the slice: x: 2, y: 2, z: 4, core: 2. Of those that a mesh axis runs over, the one named last changes fastest.
Arguments:
- target: bfloat16 [56, 2048], P('sp'), may hold values from -6 to 6
- source: bfloat16 [2048, 2048], P('sp'), may hold values from -6 to 6
- tgt_gain: float32 [2, 2048], replicated, may hold values from 0.1 to 1.9
- src_gain: float32 [2, 2048], replicated, may hold values from 0.1 to 1.9
- w_query: bfloat16 [2, 2048, 2048], P(None, None, 'tp'), may hold values from -0.125 to 0.125
- w_key: bfloat16 [2, 2048, 2048], P(None, None, 'tp'), may hold values from -0.125 to 0.125
- w_value: bfloat16 [2, 2048, 2048], P(None, None, 'tp'), may hold values from -0.125 to 0.125
- w_out: bfloat16 [2, 2048, 2048], P(None, 'tp'), may hold values from -0.125 to 0.125
- score_scale: float32 [2, 8], P(None, 'tp'), may hold values from 1.5 to 4
Outputs:
- result: bfloat16 [56, 2048], P('sp')
All inputs are finite; a program needn't handle non-finite values.
Results may differ from a plain program's by a relative error of at most 0.015.
Values may be sent and summed in bfloat16 or wider, within the bound.
A program may use at most 64 MiB of HBM per device.

v0:
```python
import math

import jax
import jax.numpy as jnp
from jax import lax
from jax.sharding import PartitionSpec as P

HEAD_DIM = 256


EPS = 1e-06


def row_scale(values):
    return lax.rsqrt(jnp.mean(values * values, axis=-1, keepdims=True) + EPS)


def head_norm(projected):
    heads = projected.reshape(projected.shape[0], -1, HEAD_DIM)
    heads = heads * row_scale(heads)
    return heads.reshape(projected.shape).astype(jnp.bfloat16)


def source_side(src_float, src_scale, gain_row, key_weight, value_weight):
    normed_src = (src_float * src_scale * gain_row).astype(jnp.bfloat16)
    key_rows = head_norm(jnp.dot(normed_src, key_weight, preferred_element_type=jnp.float32))
    value_rows = jnp.dot(normed_src, value_weight, preferred_element_type=jnp.float32).astype(
        jnp.bfloat16
    )
    return (key_rows, value_rows)


def attend(queries, key_rows, value_rows, scales):
    root = math.sqrt(HEAD_DIM)
    count = queries.shape[0]
    local_heads = scales.shape[0]
    query_heads = queries.reshape(count, local_heads, HEAD_DIM)
    key_heads = key_rows.reshape(key_rows.shape[0], local_heads, HEAD_DIM)
    value_heads = value_rows.reshape(value_rows.shape[0], local_heads, HEAD_DIM)
    scores = jnp.einsum("qhd,khd->hqk", query_heads, key_heads, preferred_element_type=jnp.float32)
    logits = scales[:, None, None] * (scores / root - root)
    weights = jnp.exp(logits)
    denominators = jnp.sum(weights, axis=2).T
    numerators = jnp.einsum(
        "hqk,khd->qhd",
        weights.astype(jnp.bfloat16),
        value_heads,
        preferred_element_type=jnp.float32,
    )
    return (numerators.reshape(count, local_heads * HEAD_DIM), denominators)


def place(terms):
    numer_all = terms[0]
    denom_all = terms[1]
    return (numer_all, denom_all)


def body(target, source, tgt_gain, src_gain, w_query, w_key, w_value, w_out, score_scale):
    local_heads = w_query.shape[2] // HEAD_DIM
    width = local_heads * HEAD_DIM
    tok_rows = target.shape[0]
    layer_count = w_query.shape[0]
    src_float = source.astype(jnp.float32)
    src_scale = row_scale(src_float)
    hidden = target
    for layer_index in range(layer_count):
        key_rows, value_rows = source_side(
            src_float, src_scale, src_gain[layer_index], w_key[layer_index], w_value[layer_index]
        )
        scales = score_scale[layer_index]
        hidden_float = hidden.astype(jnp.float32)
        normed_tgt = (hidden_float * row_scale(hidden_float) * tgt_gain[layer_index]).astype(
            jnp.bfloat16
        )
        weight_now = w_query[layer_index]
        query_rows = head_norm(jnp.dot(normed_tgt, weight_now, preferred_element_type=jnp.float32))
        running = place(
            attend(
                lax.all_gather(query_rows, "sp", axis=0, tiled=True), key_rows, value_rows, scales
            )
        )
        numerators, denominators = (
            lax.psum_scatter(running[0], "sp", scatter_dimension=0, tiled=True),
            lax.psum_scatter(running[1], "sp", scatter_dimension=0, tiled=True),
        )
        attended = (
            (numerators.reshape(tok_rows, local_heads, HEAD_DIM) / denominators[:, :, None])
            .reshape(tok_rows, width)
            .astype(jnp.bfloat16)
        )
        share = jnp.dot(attended, w_out[layer_index], preferred_element_type=jnp.float32).astype(
            jnp.bfloat16
        )
        branch = lax.psum(share.astype(jnp.float32).astype(jnp.bfloat16), "tp").astype(jnp.float32)
        hidden = (hidden_float + branch).astype(jnp.bfloat16)
    return hidden


def solution(mesh):
    placed = (
        P("sp", None),
        P("sp", None),
        P(),
        P(),
        P(None, None, "tp"),
        P(None, None, "tp"),
        P(None, None, "tp"),
        P(None, "tp", None),
        P(None, "tp"),
    )
    return jax.shard_map(body, mesh=mesh, in_specs=placed, out_specs=P("sp", None), check_vma=False)
```

profile of v0, /device:TPU:0, one launch (start us, length us, event | category | flops | bytes accessed | tf_op | source)
XLA Modules:
  0.0 235.5 jit_solution(8419340724434277195)
XLA Ops:
  0.0 1.5 fusion.6
  1.5 0.8 fusion.73
  2.3 3.8 %slice_bitcast_fusion.2 = (bf16[512,2048]{0,1:T(8,128)(2,1)S(1)}, bf16[512,2048]{0,1:T(8,128)(2,1)}) fusion(bf16[2,2048,512]{2,1,0:T(8,128)(2,1)} %param.14), kind=kLoop, calls=%fused_computation.20 | loop fusion | bytes 8388608 | tf_op jit(solution)/shard_map/dot_general | solution.py:26
  6.2 2.5 %copy.31 = bf16[512,2048]{1,0:T(8,128)(2,1)} copy(bf16[512,2048]{0,1:T(8,128)(2,1)S(1)} %get-tuple-element.7) | data formatting | bytes 4194304 | tf_op jit(solution)/shard_map/dot_general | solution.py:26
  8.6 3.4 %multiply_reduce_fusion.1 = (f32[256,2]{0,1:T(2,128)S(1)}, f32[256,2,256]{0,2,1:T(8,128)}) fusion(bf16[2,256,2048]{2,1,0:T(8,128)(2,1)} %bitcast.104, f32[2048]{0:T(1024)S(1)} %bitcast.117, f32[256]{0:T(256)S(1)} %add_rsqrt_fusion.4, bf16[256,2048]{1,0:T(8,128)(2,1)S(1)} %copy-done.3), kind=kOutput, calls=%fused_computation.42 | convolution fusion | flops 539229696 | bytes 3681280 | tf_op jit(solution)/shard_map/dot_general | solution.py:26
  12.0 2.3 slice_bitcast_fusion.3
  14.3 2.9 %copy.30 = bf16[512,2048]{1,0:T(8,128)(2,1)S(1)} copy(bf16[512,2048]{0,1:T(8,128)(2,1)} %get-tuple-element.5) | data formatting | bytes 4194304 | tf_op jit(solution)/shard_map/dot_general | solution.py:77
  17.5 0.7 multiply_reduce_fusion.3
  18.3 32.4 %all-gather = bf16[8,7,512]{2,1,0:T(8,128)(2,1)S(1)} all-gather(bf16[1,7,512]{2,1,0:T(8,128)(2,1)S(1)} %bitcast.113), channel_id=1, replica_groups=mesh['sp'=8,'tp'=4] {'sp'}, dimensions={0}, use_global_device_ids=true | all-gather | bytes 64512 | tf_op jit(solution)/shard_map/all_gather | solution.py:80
  50.7 2.5 %fusion.17 = bf16[256,512]{1,0:T(8,128)(2,1)S(1)} fusion(bf16[2,2048,512]{2,1,0:T(8,128)(2,1)} %param.15, bf16[256,2048]{1,0:T(8,128)(2,1)S(1)} %copy-done.3, f32[2048]{0:T(1024)S(1)} %bitcast.118, f32[256]{0:T(256)S(1)} %add_rsqrt_fusion.4), kind=kOutput, calls=%fused_computation.23 | convolution fusion | flops 539099136 | bytes 3417088 | tf_op jit(solution)/shard_map/dot_general | solution.py:27
  53.2 0.3 fusion.75
  53.5 0.2 convolution_bitcast_fusion.1
  53.7 22.6 %fusion = f32[8,512]{1,0:T(8,128)S(1)} fusion(f32[56,512]{1,0:T(8,128)S(1)} %bitcast.105), kind=kCustom, calls=%all-reduce-scatter | all-reduce-scatter fusion | flops 32769 | bytes 131584
  76.3 1.3 collective-permute-start
  77.7 33.7 %all-reduce.1 = f32[56,2]{1,0:T(8,128)S(1)} all-reduce(f32[56,2]{1,0:T(8,128)S(1)} %copy.36), channel_id=3, replica_groups=mesh['sp'=8,'tp'=4] {'sp'}, use_global_device_ids=true, to_apply=%region_6.0.clone | all-reduce | flops 112 | bytes 896
  111.4 0.6 fusion.74
  112.7 2.5 %copy.38 = bf16[512,2048]{1,0:T(8,128)(2,1)} copy(bf16[512,2048]{0,1:T(8,128)(2,1)S(1)} %copy-done) | data formatting | bytes 4194304 | tf_op jit(solution)/shard_map/dot_general | solution.py:26
  115.2 2.5 %fusion.20 = bf16[256,512]{1,0:T(8,128)(2,1)S(1)} fusion(bf16[2,2048,512]{2,1,0:T(8,128)(2,1)} %param.15, bf16[256,2048]{1,0:T(8,128)(2,1)S(1)} %copy-done.3, f32[2048]{0:T(1024)S(1)} %bitcast.115, f32[256]{0:T(256)S(1)} %add_rsqrt_fusion.4), kind=kOutput, calls=%fused_computation.24 | convolution fusion | flops 539099136 | bytes 3417088 | tf_op jit(solution)/shard_map/dot_general | solution.py:27
  117.7 1.6 multiply_reduce_fusion
  120.0 2.9 %copy.37 = bf16[512,2048]{1,0:T(8,128)(2,1)S(1)} copy(bf16[512,2048]{0,1:T(8,128)(2,1)} %get-tuple-element.6) | data formatting | bytes 4194304 | tf_op jit(solution)/shard_map/dot_general | solution.py:77
  123.1 2.0 convolution_convert_fusion.1
  125.1 10.3 %psum.14 = bf16[7,2048]{1,0:T(8,128)(2,1)S(1)} all-reduce(bf16[7,2048]{1,0:T(8,128)(2,1)S(1)} %convolution_convert_fusion.1), channel_id=1, replica_groups=mesh['sp'=8,'tp'=4] {'tp'}, use_global_device_ids=true, to_apply=%region_7.0 | all-reduce | flops 14336 | bytes 57344 | tf_op jit(solution)/shard_map/psum | solution.py:95
  135.5 0.7 multiply_reduce_fusion.2
  136.3 30.5 %all-gather.1 = bf16[8,7,512]{2,1,0:T(8,128)(2,1)S(1)} all-gather(bf16[1,7,512]{2,1,0:T(8,128)(2,1)S(1)} %bitcast.114), channel_id=1, replica_groups=mesh['sp'=8,'tp'=4] {'sp'}, dimensions={0}, use_global_device_ids=true | all-gather | bytes 64512 | tf_op jit(solution)/shard_map/all_gather | solution.py:80
  166.9 0.3 fusion.76
  167.2 0.2 convolution_bitcast_fusion
  167.4 19.9 %fusion.1 = f32[8,512]{1,0:T(8,128)S(1)} fusion(f32[56,512]{1,0:T(8,128)S(1)} %bitcast.106), kind=kCustom, calls=%all-reduce-scatter.1 | all-reduce-scatter fusion | flops 32769 | bytes 131584
  187.3 1.9 collective-permute-start.1
  189.3 33.1 %all-reduce.3 = f32[56,2]{1,0:T(8,128)S(1)} all-reduce(f32[56,2]{1,0:T(8,128)S(1)} %copy.43), channel_id=5, replica_groups=mesh['sp'=8,'tp'=4] {'sp'}, use_global_device_ids=true, to_apply=%region_13.0.clone | all-reduce | flops 112 | bytes 896
  222.6 2.0 convolution_convert_fusion
  224.6 10.3 %psum.15 = bf16[7,2048]{1,0:T(8,128)(2,1)S(1)} all-reduce(bf16[7,2048]{1,0:T(8,128)(2,1)S(1)} %convolution_convert_fusion), channel_id=1, replica_groups=mesh['sp'=8,'tp'=4] {'tp'}, use_global_device_ids=true, to_apply=%region_14.0 | all-reduce | flops 14336 | bytes 57344 | tf_op jit(solution)/shard_map/psum | solution.py:95
  234.9 0.6 fusion.50
  (51 shorter events, 1.2 us)
Async XLA Ops:
  6.2 2.5 %copy-start.3 = (bf16[256,2048]{1,0:T(8,128)(2,1)S(1)}, bf16[256,2048]{1,0:T(8,128)(2,1)}, u32[]{:S(2)}) copy-start(bf16[256,2048]{1,0:T(8,128)(2,1)} %param.10) | copy-start | bytes 3145732
  8.6 3.4 %copy-start.1 = (bf16[2,2048,512]{2,1,0:T(8,128)(2,1)S(1)}, bf16[2,2048,512]{2,1,0:T(8,128)(2,1)}, u32[]{:S(2)}) copy-start(bf16[2,2048,512]{2,1,0:T(8,128)(2,1)} %param.13) | copy-start | bytes 12582916
  14.3 3.0 %copy-start.7 = (f32[2,2048]{1,0:T(2,128)S(1)}, f32[2,2048]{1,0:T(2,128)}, u32[]{:S(2)}) copy-start(f32[2,2048]{1,0:T(2,128)} %param.11) | copy-start | bytes 49156
  14.3 3.0 %copy-start.4 = (bf16[7,2048]{1,0:T(8,128)(2,1)S(1)}, bf16[7,2048]{1,0:T(8,128)(2,1)}, u32[]{:S(2)}) copy-start(bf16[7,2048]{1,0:T(8,128)(2,1)} %param.9) | copy-start | bytes 86020
  17.3 33.4 %copy-start.9 = (f32[2,2]{1,0:T(2,128)S(1)}, f32[2,2]{1,0:T(2,128)}, u32[]{:S(2)}) copy-start(f32[2,2]{1,0:T(2,128)} %param.17) | copy-start | bytes 52
  50.7 2.5 %copy-start.6 = (f32[256,2,256]{0,2,1:T(8,128)S(1)}, f32[256,2,256]{0,2,1:T(8,128)}, u32[]{:S(2)}) copy-start(f32[256,2,256]{0,2,1:T(8,128)} %get-tuple-element.20) | copy-start | bytes 1572868
  50.7 60.7 %copy-start.8 = (u32[32]{0:T(128)S(1)}, u32[32]{0:T(128)}, u32[]{:S(2)}) copy-start(u32[32]{0:T(128)} %constant.31) | copy-start | bytes 388
  50.7 62.0 %copy-start = (bf16[512,2048]{0,1:T(8,128)(2,1)S(1)}, bf16[512,2048]{0,1:T(8,128)(2,1)}, u32[]{:S(2)}) copy-start(bf16[512,2048]{0,1:T(8,128)(2,1)} %get-tuple-element.8) | copy-start | bytes 6291460
  76.3 46.7 %collective-permute-start = (f32[7,512]{1,0:T(8,128)S(1)}, f32[7,512]{1,0:T(8,128)S(1)}, u32[]{:S(2)}, u32[]{:S(2)}) collective-permute-start(f32[7,512]{1,0:T(8,128)S(1)} %slice.56), channel_id=1, source_target_pairs={{0,4},{4,8},{8,12},{12,16},{16,20},{20,24},{24,28},{1,5},{5,9},{9,... | collective-permute-start | bytes 43016
  115.2 2.5 %copy-start.2 = (bf16[512,2048]{1,0:T(8,128)(2,1)S(1)}, bf16[512,2048]{1,0:T(8,128)(2,1)}, u32[]{:S(2)}) copy-start(bf16[512,2048]{1,0:T(8,128)(2,1)} %copy.38) | copy-start | bytes 6291460
  123.1 43.9 %copy-start.5 = (f32[256,2,256]{0,2,1:T(8,128)S(1)}, f32[256,2,256]{0,2,1:T(8,128)}, u32[]{:S(2)}) copy-start(f32[256,2,256]{0,2,1:T(8,128)} %get-tuple-element.18) | copy-start | bytes 1572868
  187.3 35.2 %collective-permute-start.1 = (f32[7,512]{1,0:T(8,128)S(1)}, f32[7,512]{1,0:T(8,128)S(1)}, u32[]{:S(2)}, u32[]{:S(2)}) collective-permute-start(f32[7,512]{1,0:T(8,128)S(1)} %slice.57), channel_id=1, source_target_pairs={{0,4},{4,8},{8,12},{12,16},{16,20},{20,24},{24,28},{1,5},{5,9},{9,... | collective-permute-start | bytes 43016
where the time goes:
time: 236 us; the launch traced here: 235 us
  blocking collectives  193 us (82%)
  local copies, waits for them, and re-layouts  19.1 us (8%)
  matrix products  16.3 us (7%)
  starting transfers between devices  3.19 us (1%)
  other arithmetic  2.62 us (1%)
    unnamed x4, blocking collectives  109 us
    all_gather x2, blocking collectives, body(): lax.all_gather(query_rows, 'sp', axis=0, tiled=True)  62.9 us
    psum x2, blocking collectives, body(): lax.psum(share.astype(jnp.float32).astype(jnp.bfloat16), 'tp')  20.5 us
    dot_general x3, local copies, waits for them, and re-layouts, source_side(): jnp.dot(normed_src, key_weight, preferred_element_type=jnp.float32)  8.79 us
    dot_general x3, local copies, waits for them, and re-layouts, body(): jnp.dot(normed_tgt, weight_now, preferred_element_type=jnp.float32)  8.14 us
    dot_general x2, matrix products, source_side(): jnp.dot(normed_src, key_weight, preferred_element_type=jnp.float32)  4.99 us
    dot_general x2, matrix products, source_side(): jnp.dot(normed_src, value_weight, preferred_element_type=jnp.float32)  4.98 us
  transfers between devices with their start and end apart: 2, of which 0 were waited for; matrix products, arithmetic and copies ran while one was open for 4% of the time, Pallas kernels for 0%

commit v1 on v0

v1 whole, which is shorter than its diff:
```python
import functools
import math

import jax
import jax.numpy as jnp
from jax import lax
from jax.experimental import pallas as pl
from jax.experimental.pallas import tpu as pltpu
from jax.sharding import PartitionSpec as P

HEAD_DIM = 256
EPS = 1e-06
LANES = 128
SUBLANES = 8
MESH = pl.DeviceIdType.MESH
BF16 = jnp.bfloat16
F32 = jnp.float32


def row_scale(values):
    return lax.rsqrt(jnp.mean(values * values, axis=-1, keepdims=True) + EPS)


def each(count, step):
    if count <= 8:
        for index in range(count):
            step(index)
    else:

        def turn(index, carry):
            step(index)
            return carry

        lax.fori_loop(0, count, turn, 0)


def kernel(
    n_sp,
    n_tp,
    target,
    source,
    tgt_gain,
    src_gain,
    w_query,
    w_key,
    w_value,
    w_out,
    score_scale,
    out,
    tgt_v,
    src_v,
    tg_v,
    sg_v,
    wq_v,
    wk_v,
    wv_v,
    wo_v,
    scale_s,
    out_v,
    hid,
    normed,
    keys,
    vals,
    q_all,
    num_send,
    num_recv,
    shares,
    load_sem,
    w_sem,
    send_sem,
    recv_sem,
):
    layers = w_query.shape[0]
    rows = target.shape[0]
    pad = hid.shape[0]
    width = w_query.shape[2]
    heads = width // HEAD_DIM
    src_rows = source.shape[0]
    root = math.sqrt(HEAD_DIM)
    me_s = lax.axis_index("sp")
    me_t = lax.axis_index("tp")

    def sp_peer(step):
        return lax.rem(me_s + step + 1, n_sp)

    def tp_peer(step):
        return lax.rem(me_t + step + 1, n_tp)

    small = [
        pltpu.make_async_copy(target, tgt_v, load_sem.at[0]),
        pltpu.make_async_copy(tgt_gain, tg_v, load_sem.at[1]),
        pltpu.make_async_copy(src_gain, sg_v, load_sem.at[2]),
        pltpu.make_async_copy(score_scale, scale_s, load_sem.at[3]),
        pltpu.make_async_copy(source, src_v, load_sem.at[4]),
    ]
    big = {}
    for layer in range(layers):
        for kind, (hbm, vmem) in enumerate(
            ((w_query, wq_v), (w_key, wk_v), (w_value, wv_v), (w_out, wo_v))
        ):
            big[layer, kind] = pltpu.make_async_copy(
                hbm.at[layer], vmem.at[layer], w_sem.at[layer, kind]
            )
    for copy in small:
        copy.start()
    big[0, 0].start()
    big[0, 1].start()
    big[0, 2].start()

    barrier = pltpu.get_barrier_semaphore()

    def greet_sp(step):
        pl.semaphore_signal(
            barrier, inc=1, device_id={"sp": sp_peer(step)}, device_id_type=MESH
        )

    def greet_tp(step):
        pl.semaphore_signal(
            barrier, inc=1, device_id={"tp": tp_peer(step)}, device_id_type=MESH
        )

    each(n_sp - 1, greet_sp)
    each(n_tp - 1, greet_tp)

    def remote(src, dst, stage, layer, target_id):
        return pltpu.make_async_remote_copy(
            src_ref=src,
            dst_ref=dst,
            send_sem=send_sem.at[layer, stage],
            recv_sem=recv_sem.at[layer, stage],
            device_id=target_id,
            device_id_type=MESH,
        )

    def wait_bytes(ref, sem):
        pltpu.make_async_copy(ref, ref, sem).wait()

    def head_norm(block):
        return (block * row_scale(block)).astype(BF16)

    def make_queries(layer):
        hidden = hid[...]
        normed_tgt = (hidden * row_scale(hidden) * tg_v[layer : layer + 1, :]).astype(BF16)
        for head in range(heads):
            cols = slice(head * HEAD_DIM, (head + 1) * HEAD_DIM)
            block = jnp.dot(normed_tgt, wq_v[layer, :, cols], preferred_element_type=F32)
            q_all[layer, me_s, :, cols] = head_norm(block)

    def send_queries(layer):
        def go(step):
            remote(
                q_all.at[layer, me_s], q_all.at[layer, me_s], 0, layer, {"sp": sp_peer(step)}
            ).start()

        each(n_sp - 1, go)

    def make_source(layer):
        rows_in = normed[layer]
        big[layer, 1].wait()
        for head in range(heads):
            cols = slice(head * HEAD_DIM, (head + 1) * HEAD_DIM)
            block = jnp.dot(rows_in, wk_v[layer, :, cols], preferred_element_type=F32)
            keys[layer, head] = head_norm(block)
        big[layer, 2].wait()
        for head in range(heads):
            cols = slice(head * HEAD_DIM, (head + 1) * HEAD_DIM)
            block = jnp.dot(rows_in, wv_v[layer, :, cols], preferred_element_type=F32)
            vals[layer, head] = block.astype(BF16)

    chunk = math.gcd(n_sp, 8)
    count = chunk * pad

    def attend(layer):
        def one(step):
            first = step * chunk
            lane = lax.broadcasted_iota(jnp.int32, (count, LANES), 1)
            extra = jnp.zeros((count, LANES), F32)
            queries = q_all[layer, pl.ds(first, chunk)].astype(F32).reshape(count, width)
            for head in range(heads):
                cols = slice(head * HEAD_DIM, (head + 1) * HEAD_DIM)
                scores = lax.dot_general(
                    queries[:, cols].astype(BF16),
                    keys[layer, head],
                    (((1,), (1,)), ((), ())),
                    preferred_element_type=F32,
                )
                weights = jnp.exp(scale_s[layer, head] * (scores / root - root))
                denom = jnp.sum(weights, axis=1, keepdims=True)
                high = denom.astype(BF16).astype(F32)
                extra = jnp.where(lane == 2 * head, high, extra)
                extra = jnp.where(lane == 2 * head + 1, denom - high, extra)
                numer = jnp.dot(
                    weights.astype(BF16), vals[layer, head], preferred_element_type=F32
                )
                num_send[layer, pl.ds(first, chunk), :, cols] = numer.reshape(
                    chunk, pad, HEAD_DIM
                ).astype(BF16)
            num_send[layer, pl.ds(first, chunk), :, width:] = extra.reshape(
                chunk, pad, LANES
            ).astype(BF16)

        each(n_sp // chunk, one)

    def send_numerators(layer):
        def go(step):
            peer = sp_peer(step)
            remote(
                num_send.at[layer, peer], num_recv.at[layer, me_s], 1, layer, {"sp": peer}
            ).start()

        each(n_sp - 1, go)
        num_recv[layer, me_s] = num_send[layer, me_s]

    def finish_attention(layer):
        wait_bytes(num_recv.at[layer, pl.ds(0, n_sp - 1)], recv_sem.at[layer, 1])
        total = jnp.sum(num_recv[layer].astype(F32), axis=0)
        pieces = []
        for head in range(heads):
            cols = slice(head * HEAD_DIM, (head + 1) * HEAD_DIM)
            at = width + 2 * head
            denom = total[:, at : at + 1] + total[:, at + 1 : at + 2]
            pieces.append((total[:, cols] / denom).astype(BF16))
        return pieces

    def send_shares(layer, pieces):
        acc = None
        for head in range(heads):
            part = jnp.dot(
                pieces[head],
                wo_v[layer, head * HEAD_DIM : (head + 1) * HEAD_DIM, :],
                preferred_element_type=F32,
            )
            acc = part if acc is None else acc + part
        shares[layer, me_t] = acc.astype(BF16)

        def go(step):
            remote(
                shares.at[layer, me_t], shares.at[layer, me_t], 2, layer, {"tp": tp_peer(step)}
            ).start()

        each(n_tp - 1, go)

    small[0].wait()
    small[1].wait()
    hid[...] = jnp.zeros_like(hid)
    hid[0:rows, :] = tgt_v[...].astype(F32)
    big[0, 0].wait()
    make_queries(0)
    for layer in range(layers):
        for kind in (1, 2, 3, 0):
            if (layer, kind) not in ((0, 0), (0, 1), (0, 2)):
                big[layer, kind].start()
    pl.semaphore_wait(barrier, n_sp - 1 + n_tp - 1)
    send_queries(0)

    small[2].wait()
    small[4].wait()
    step_rows = math.gcd(src_rows, 16)

    def norm_rows(index, carry):
        at = pl.ds(pl.multiple_of(index * step_rows, step_rows), step_rows)
        block = src_v[at, :].astype(F32)
        block = block * row_scale(block)
        for layer in range(layers):
            normed[layer, at, :] = (block * sg_v[layer : layer + 1, :]).astype(BF16)
        return carry

    lax.fori_loop(0, src_rows // step_rows, norm_rows, 0)
    small[3].wait()
    for layer in range(layers):
        make_source(layer)

    for layer in range(layers):
        if layer > 0:
            big[layer, 0].wait()
            make_queries(layer)
            send_queries(layer)
        wait_bytes(q_all.at[layer, pl.ds(0, n_sp - 1)], recv_sem.at[layer, 0])
        attend(layer)
        send_numerators(layer)
        big[layer, 3].wait()
        send_shares(layer, finish_attention(layer))
        wait_bytes(shares.at[layer, pl.ds(0, n_tp - 1)], recv_sem.at[layer, 2])
        branch = jnp.sum(shares[layer].astype(F32), axis=0)
        hid[...] = (hid[...] + branch).astype(BF16).astype(F32)

    out_v[...] = hid[0:rows, :].astype(BF16)
    final = pltpu.make_async_copy(out_v, out, load_sem.at[5])
    final.start()
    for layer in range(layers):
        wait_bytes(q_all.at[layer, pl.ds(0, n_sp - 1)], send_sem.at[layer, 0])
        wait_bytes(num_recv.at[layer, pl.ds(0, n_sp - 1)], send_sem.at[layer, 1])
        wait_bytes(shares.at[layer, pl.ds(0, n_tp - 1)], send_sem.at[layer, 2])
    final.wait()


def solution(mesh):
    n_sp, n_tp = mesh.shape["sp"], mesh.shape["tp"]
    placed = (
        P("sp", None),
        P("sp", None),
        P(),
        P(),
        P(None, None, "tp"),
        P(None, None, "tp"),
        P(None, None, "tp"),
        P(None, "tp", None),
        P(None, "tp"),
    )

    def body(*args):
        target, source, tgt_gain, src_gain, w_query, w_key, w_value, w_out, score_scale = args
        layers, model, width = w_query.shape
        rows = target.shape[0]
        src_rows = source.shape[0]
        heads = width // HEAD_DIM
        pad = -(-rows // SUBLANES) * SUBLANES
        anywhere = pl.BlockSpec(memory_space=pl.ANY)
        return pl.pallas_call(
            functools.partial(kernel, n_sp, n_tp),
            out_shape=jax.ShapeDtypeStruct(target.shape, BF16),
            in_specs=[anywhere] * len(args),
            out_specs=anywhere,
            scratch_shapes=[
                pltpu.VMEM(target.shape, BF16),
                pltpu.VMEM(source.shape, BF16),
                pltpu.VMEM(tgt_gain.shape, F32),
                pltpu.VMEM(src_gain.shape, F32),
                pltpu.VMEM(w_query.shape, BF16),
                pltpu.VMEM(w_key.shape, BF16),
                pltpu.VMEM(w_value.shape, BF16),
                pltpu.VMEM(w_out.shape, BF16),
                pltpu.SMEM(score_scale.shape, F32),
                pltpu.VMEM(target.shape, BF16),
                pltpu.VMEM((pad, model), F32),
                pltpu.VMEM((layers, src_rows, model), BF16),
                pltpu.VMEM((layers, heads, src_rows, HEAD_DIM), BF16),
                pltpu.VMEM((layers, heads, src_rows, HEAD_DIM), BF16),
                pltpu.VMEM((layers, n_sp, pad, width), BF16),
                pltpu.VMEM((layers, n_sp, pad, width + LANES), BF16),
                pltpu.VMEM((layers, n_sp, pad, width + LANES), BF16),
                pltpu.VMEM((layers, n_tp, pad, model), BF16),
                pltpu.SemaphoreType.DMA((6,)),
                pltpu.SemaphoreType.DMA((layers, 4)),
                pltpu.SemaphoreType.DMA((layers, 3)),
                pltpu.SemaphoreType.DMA((layers, 3)),
            ],
            compiler_params=pltpu.CompilerParams(
                collective_id=0, has_side_effects=True, vmem_limit_bytes=60 * 1024 * 1024
            ),
        )(*args)

    return jax.shard_map(
        body, mesh=mesh, in_specs=placed, out_specs=P("sp", None), check_vma=False
    )
```

time: 236 us -> 34.5 us (0.15)
  blocking collectives: 193 us -> 0 us
  Pallas kernels: 0 us -> 32.9 us
  local copies, waits for them, and re-layouts: 19.1 us -> 1.38 us
  matrix products: 16.3 us -> 0 us
  starting transfers between devices: 3.19 us -> 0 us
  other arithmetic: 2.62 us -> 0 us
    unnamed x4 -> x0, blocking collectives: 109 us -> none
    all_gather x2 -> x0, blocking collectives: 62.9 us -> none  [body(): lax.all_gather(query_rows, 'sp', axis=0, tiled=True)]
    pallas_call x0 -> x1, Pallas kernels: none -> 32.9 us  [body(): pl.pallas_call(functools.partial(kernel, n_sp, n_tp), out_shape=jax.Shape...]
    psum x2 -> x0, blocking collectives: 20.5 us -> none  [body(): lax.psum(share.astype(jnp.float32).astype(jnp.bfloat16), 'tp')]
    dot_general x6 -> x0, local copies, waits for them, and re-layouts: 16.9 us -> none  [the longest x3 8.79 us: source_side(): jnp.dot(normed_src, key_weight, preferred_element_type=jnp.float32)]
    dot_general x12 -> x0, matrix products: 16.3 us -> none  [the longest x2 4.99 us: source_side(): jnp.dot(normed_src, key_weight, preferred_element_type=jnp.float32)]
    unnamed x2 -> x0, starting transfers between devices: 3.19 us -> none
  transfers between devices with their start and end apart: 2 -> 0, of which waited for: 0 -> 0; matrix products, arithmetic and copies ran while one was open for 4% -> 0% of each run, Pallas kernels for 0% -> 0%
where the time goes in v1:
time: 34.5 us; the launch traced here: 34.3 us
  Pallas kernels  32.9 us (95%)
  local copies, waits for them, and re-layouts  1.38 us (4%)
    pallas_call x1, Pallas kernels, body(): pl.pallas_call(functools.partial(kernel, n_sp, n_tp), out_shape=jax.Shape...  32.9 us
    unnamed x1, local copies, waits for them, and re-layouts  1.38 us

profile of v1, /device:TPU:0, one launch (start us, length us, event | category | flops | bytes accessed | tf_op | source)
XLA Modules:
  0.0 34.3 jit_solution(10010032954262100410)
XLA Ops:
  0.0 32.9 %shard_map.91 = bf16[7,2048]{1,0:T(8,128)(2,1)} custom-call(bf16[7,2048]{1,0:T(8,128)(2,1)} %target.1, bf16[256,2048]{1,0:T(8,128)(2,1)} %source.1, f32[2,2048]{1,0:T(2,128)} %tgt_gain.1, f32[2,2048]{1,0:T(2,128)} %src_gain.1, bf16[2,2048,512]{2,1,0:T(8,128)(2,1)} %w_query.1, bf16[2,2048,512]{2,1,0:T(8,128)(2,1)} %w_key.1, bf16[2,2048,512]{2,1,0:T(8,128)(2,1)} %w_value.1, ...), custom_call_target="tpu_custom_call" | custom-call | tf_op jit(solution)/shard_map/pallas_call | solution.py:319
  32.9 1.4 %copy.11 = bf16[7,2048]{1,0:T(8,128)(2,1)} copy(bf16[7,2048]{1,0:T(8,128)(2,1)} %shard_map.91) | data formatting | bytes 57344

commit v2 on v1

--- a/solution.py
+++ b/solution.py
@@ -257,18 +257,19 @@
     small[4].wait()
     step_rows = math.gcd(src_rows, 16)
 
-    def norm_rows(index, carry):
-        at = pl.ds(pl.multiple_of(index * step_rows, step_rows), step_rows)
-        block = src_v[at, :].astype(F32)
-        block = block * row_scale(block)
-        for layer in range(layers):
-            normed[layer, at, :] = (block * sg_v[layer : layer + 1, :]).astype(BF16)
-        return carry
-
-    lax.fori_loop(0, src_rows // step_rows, norm_rows, 0)
+    def norm_source(layer):
+        def norm_rows(index, carry):
+            at = pl.ds(pl.multiple_of(index * step_rows, step_rows), step_rows)
+            block = src_v[at, :].astype(F32)
+            block = block * row_scale(block) * sg_v[layer : layer + 1, :]
+            normed[layer, at, :] = block.astype(BF16)
+            return carry
+
+        lax.fori_loop(0, src_rows // step_rows, norm_rows, 0)
+
+    norm_source(0)
     small[3].wait()
-    for layer in range(layers):
-        make_source(layer)
+    make_source(0)
 
     for layer in range(layers):
         if layer > 0:
@@ -278,6 +279,9 @@
         wait_bytes(q_all.at[layer, pl.ds(0, n_sp - 1)], recv_sem.at[layer, 0])
         attend(layer)
         send_numerators(layer)
+        if layer + 1 < layers:
+            norm_source(layer + 1)
+            make_source(layer + 1)
         big[layer, 3].wait()
         send_shares(layer, finish_attention(layer))
         wait_bytes(shares.at[layer, pl.ds(0, n_tp - 1)], recv_sem.at[layer, 2])

time: 34.5 us -> 33.6 us (0.974)
  Pallas kernels: 32.9 us -> 32.1 us
    pallas_call x1, Pallas kernels: 32.9 us -> 32.1 us  [body(): pl.pallas_call(functools.partial(kernel, n_sp, n_tp), out_shape=jax.Shape...]
where the time goes in v2:
time: 33.6 us; the launch traced here: 33.5 us
  Pallas kernels  32.1 us (96%)
  local copies, waits for them, and re-layouts  1.38 us (4%)
    pallas_call x1, Pallas kernels, body(): pl.pallas_call(functools.partial(kernel, n_sp, n_tp), out_shape=jax.Shape...  32.1 us
    unnamed x1, local copies, waits for them, and re-layouts  1.38 us

profile of v2, /device:TPU:0, one launch (start us, length us, event | category | flops | bytes accessed | tf_op | source)
XLA Modules:
  0.0 33.5 jit_solution(5644461996687190784)
XLA Ops:
  0.0 32.1 %shard_map.91 = bf16[7,2048]{1,0:T(8,128)(2,1)} custom-call(bf16[7,2048]{1,0:T(8,128)(2,1)} %target.1, bf16[256,2048]{1,0:T(8,128)(2,1)} %source.1, f32[2,2048]{1,0:T(2,128)} %tgt_gain.1, f32[2,2048]{1,0:T(2,128)} %src_gain.1, bf16[2,2048,512]{2,1,0:T(8,128)(2,1)} %w_query.1, bf16[2,2048,512]{2,1,0:T(8,128)(2,1)} %w_key.1, bf16[2,2048,512]{2,1,0:T(8,128)(2,1)} %w_value.1, ...), custom_call_target="tpu_custom_call" | custom-call | tf_op jit(solution)/shard_map/pallas_call | solution.py:323
  32.1 1.4 %copy.11 = bf16[7,2048]{1,0:T(8,128)(2,1)} copy(bf16[7,2048]{1,0:T(8,128)(2,1)} %shard_map.91) | data formatting | bytes 57344

commit v3 on v2

--- a/solution.py
+++ b/solution.py
@@ -10,7 +10,7 @@
 
 HEAD_DIM = 256
 EPS = 1e-06
-LANES = 128
+PARTS = 4
 SUBLANES = 8
 MESH = pl.DeviceIdType.MESH
 BF16 = jnp.bfloat16
@@ -67,9 +67,10 @@
     shares,
     load_sem,
     w_sem,
-    send_sem,
-    recv_sem,
+    *sems,
 ):
+    q_sems, n_sems, s_sems = sems[0:2], sems[2:4], sems[4:6]
+    parts, part_width = shares.shape[1], shares.shape[4]
     layers = w_query.shape[0]
     rows = target.shape[0]
     pad = hid.shape[0]
@@ -80,11 +81,24 @@
     me_s = lax.axis_index("sp")
     me_t = lax.axis_index("tp")
 
+    def peer_of(me, step, size):
+        if size & (size - 1):
+            return lax.rem(me + step + 1, size)
+        distance = size - 1 - step
+        peer = me
+        bit = 1
+        while bit < size:
+            here = lax.rem(me // bit, 2)
+            flip = (distance // bit) % 2
+            peer = peer + flip * bit * (1 - 2 * here)
+            bit *= 2
+        return peer
+
     def sp_peer(step):
-        return lax.rem(me_s + step + 1, n_sp)
+        return peer_of(me_s, step, n_sp)
 
     def tp_peer(step):
-        return lax.rem(me_t + step + 1, n_tp)
+        return peer_of(me_t, step, n_tp)
 
     small = [
         pltpu.make_async_copy(target, tgt_v, load_sem.at[0]),
@@ -122,12 +136,12 @@
     each(n_sp - 1, greet_sp)
     each(n_tp - 1, greet_tp)
 
-    def remote(src, dst, stage, layer, target_id):
+    def remote(src, dst, sems, at, target_id):
         return pltpu.make_async_remote_copy(
             src_ref=src,
             dst_ref=dst,
-            send_sem=send_sem.at[layer, stage],
-            recv_sem=recv_sem.at[layer, stage],
+            send_sem=sems[0].at[at],
+            recv_sem=sems[1].at[at],
             device_id=target_id,
             device_id_type=MESH,
         )
@@ -144,13 +158,15 @@
         for head in range(heads):
             cols = slice(head * HEAD_DIM, (head + 1) * HEAD_DIM)
             block = jnp.dot(normed_tgt, wq_v[layer, :, cols], preferred_element_type=F32)
-            q_all[layer, me_s, :, cols] = head_norm(block)
-
-    def send_queries(layer):
+            q_all[layer, head, me_s] = head_norm(block)
+            if layer > 0:
+                send_queries(layer, head)
+
+    def send_queries(layer, head):
+        mine = q_all.at[layer, head, me_s]
+
         def go(step):
-            remote(
-                q_all.at[layer, me_s], q_all.at[layer, me_s], 0, layer, {"sp": sp_peer(step)}
-            ).start()
+            remote(mine, mine, q_sems, (layer, head), {"sp": sp_peer(step)}).start()
 
         each(n_sp - 1, go)
 
@@ -170,75 +186,76 @@
     chunk = math.gcd(n_sp, 8)
     count = chunk * pad
 
-    def attend(layer):
+    def attend(layer, head):
         def one(step):
             first = step * chunk
-            lane = lax.broadcasted_iota(jnp.int32, (count, LANES), 1)
-            extra = jnp.zeros((count, LANES), F32)
-            queries = q_all[layer, pl.ds(first, chunk)].astype(F32).reshape(count, width)
-            for head in range(heads):
-                cols = slice(head * HEAD_DIM, (head + 1) * HEAD_DIM)
-                scores = lax.dot_general(
-                    queries[:, cols].astype(BF16),
-                    keys[layer, head],
-                    (((1,), (1,)), ((), ())),
-                    preferred_element_type=F32,
-                )
-                weights = jnp.exp(scale_s[layer, head] * (scores / root - root))
-                denom = jnp.sum(weights, axis=1, keepdims=True)
-                high = denom.astype(BF16).astype(F32)
-                extra = jnp.where(lane == 2 * head, high, extra)
-                extra = jnp.where(lane == 2 * head + 1, denom - high, extra)
-                numer = jnp.dot(
-                    weights.astype(BF16), vals[layer, head], preferred_element_type=F32
-                )
-                num_send[layer, pl.ds(first, chunk), :, cols] = numer.reshape(
-                    chunk, pad, HEAD_DIM
-                ).astype(BF16)
-            num_send[layer, pl.ds(first, chunk), :, width:] = extra.reshape(
-                chunk, pad, LANES
-            ).astype(BF16)
+            queries = q_all[layer, head, pl.ds(first, chunk)].astype(F32)
+            scores = lax.dot_general(
+                queries.reshape(count, HEAD_DIM).astype(BF16),
+                keys[layer, head],
+                (((1,), (1,)), ((), ())),
+                preferred_element_type=F32,
+            )
+            weights = jnp.exp(scale_s[layer, head] * (scores / root - root))
+            denom = jnp.sum(weights, axis=1, keepdims=True)
+            numer = jnp.dot(weights.astype(BF16), vals[layer, head], preferred_element_type=F32)
+            high = denom.astype(BF16).astype(F32).reshape(chunk, pad, 1)
+            low = denom.reshape(chunk, pad, 1) - high
+            lane = lax.broadcasted_iota(jnp.int32, (chunk, pad, HEAD_DIM), 2)
+            row = lax.broadcasted_iota(jnp.int32, (chunk, pad, HEAD_DIM), 1)
+            spread = jnp.where(lane == row, high, jnp.where(lane == row + pad, low, 0.0))
+            packed = jnp.sum(spread, axis=1, keepdims=True)
+            block = jnp.where(row == rows, packed, numer.reshape(chunk, pad, HEAD_DIM))
+            num_send[layer, head, pl.ds(first, chunk)] = block.astype(BF16)
 
         each(n_sp // chunk, one)
 
-    def send_numerators(layer):
+    def send_numerators(layer, head):
         def go(step):
             peer = sp_peer(step)
             remote(
-                num_send.at[layer, peer], num_recv.at[layer, me_s], 1, layer, {"sp": peer}
+                num_send.at[layer, head, peer],
+                num_recv.at[layer, head, me_s],
+                n_sems,
+                (layer, head),
+                {"sp": peer},
             ).start()
 
         each(n_sp - 1, go)
-        num_recv[layer, me_s] = num_send[layer, me_s]
+        num_recv[layer, head, me_s] = num_send[layer, head, me_s]
 
     def finish_attention(layer):
-        wait_bytes(num_recv.at[layer, pl.ds(0, n_sp - 1)], recv_sem.at[layer, 1])
-        total = jnp.sum(num_recv[layer].astype(F32), axis=0)
         pieces = []
-        for head in range(heads):
-            cols = slice(head * HEAD_DIM, (head + 1) * HEAD_DIM)
-            at = width + 2 * head
-            denom = total[:, at : at + 1] + total[:, at + 1 : at + 2]
-            pieces.append((total[:, cols] / denom).astype(BF16))
-        return pieces
-
-    def send_shares(layer, pieces):
-        acc = None
-        for head in range(heads):
-            part = jnp.dot(
-                pieces[head],
-                wo_v[layer, head * HEAD_DIM : (head + 1) * HEAD_DIM, :],
-                preferred_element_type=F32,
-            )
-            acc = part if acc is None else acc + part
-        shares[layer, me_t] = acc.astype(BF16)
-
-        def go(step):
-            remote(
-                shares.at[layer, me_t], shares.at[layer, me_t], 2, layer, {"tp": tp_peer(step)}
-            ).start()
-
-        each(n_tp - 1, go)
+        lane = lax.broadcasted_iota(jnp.int32, (pad, HEAD_DIM), 1)
+        row = lax.broadcasted_iota(jnp.int32, (pad, HEAD_DIM), 0)
+        mine = (lane == row) | (lane == row + pad)
+        for head in range(heads):
+            wait_bytes(num_recv.at[layer, head, pl.ds(0, n_sp - 1)], n_sems[1].at[layer, head])
+            total = jnp.sum(num_recv[layer, head].astype(F32), axis=0)
+            packed = jnp.broadcast_to(total[rows : rows + 1, :], total.shape)
+            denom = jnp.sum(jnp.where(mine, packed, 0.0), axis=1, keepdims=True)
+            pieces.append((total / denom).astype(BF16))
+        return jnp.concatenate(pieces, axis=1)
+
+    def send_shares(layer, attended):
+        for part in range(parts):
+            cols = slice(part * part_width, (part + 1) * part_width)
+            share = jnp.dot(attended, wo_v[layer, :, cols], preferred_element_type=F32)
+            shares[layer, part, me_t] = share.astype(BF16)
+            mine = shares.at[layer, part, me_t]
+
+            def go(step, mine=mine, part=part):
+                remote(mine, mine, s_sems, (layer, part), {"tp": tp_peer(step)}).start()
+
+            each(n_tp - 1, go)
+
+    def add_branch(layer):
+        for part in range(parts):
+            cols = slice(part * part_width, (part + 1) * part_width)
+            wait_bytes(shares.at[layer, part, pl.ds(0, n_tp - 1)], s_sems[1].at[layer, part])
+            branch = jnp.sum(shares[layer, part].astype(F32), axis=0)
+            total = hid[0:rows, cols] + branch[0:rows, :]
+            hid[0:rows, cols] = total.astype(BF16).astype(F32)
 
     small[0].wait()
     small[1].wait()
@@ -251,7 +268,8 @@
             if (layer, kind) not in ((0, 0), (0, 1), (0, 2)):
                 big[layer, kind].start()
     pl.semaphore_wait(barrier, n_sp - 1 + n_tp - 1)
-    send_queries(0)
+    for head in range(heads):
+        send_queries(0, head)
 
     small[2].wait()
     small[4].wait()
@@ -265,7 +283,7 @@
             normed[layer, at, :] = block.astype(BF16)
             return carry
 
-        lax.fori_loop(0, src_rows // step_rows, norm_rows, 0)
+        lax.fori_loop(0, src_rows // step_rows, norm_rows, 0, unroll=4)
 
     norm_source(0)
     small[3].wait()
@@ -275,26 +293,26 @@
         if layer > 0:
             big[layer, 0].wait()
             make_queries(layer)
-            send_queries(layer)
-        wait_bytes(q_all.at[layer, pl.ds(0, n_sp - 1)], recv_sem.at[layer, 0])
-        attend(layer)
-        send_numerators(layer)
+        for head in range(heads):
+            wait_bytes(q_all.at[layer, head, pl.ds(0, n_sp - 1)], q_sems[1].at[layer, head])
+            attend(layer, head)
+            send_numerators(layer, head)
         if layer + 1 < layers:
             norm_source(layer + 1)
             make_source(layer + 1)
         big[layer, 3].wait()
         send_shares(layer, finish_attention(layer))
-        wait_bytes(shares.at[layer, pl.ds(0, n_tp - 1)], recv_sem.at[layer, 2])
-        branch = jnp.sum(shares[layer].astype(F32), axis=0)
-        hid[...] = (hid[...] + branch).astype(BF16).astype(F32)
+        add_branch(layer)
 
     out_v[...] = hid[0:rows, :].astype(BF16)
     final = pltpu.make_async_copy(out_v, out, load_sem.at[5])
     final.start()
     for layer in range(layers):
-        wait_bytes(q_all.at[layer, pl.ds(0, n_sp - 1)], send_sem.at[layer, 0])
-        wait_bytes(num_recv.at[layer, pl.ds(0, n_sp - 1)], send_sem.at[layer, 1])
-        wait_bytes(shares.at[layer, pl.ds(0, n_tp - 1)], send_sem.at[layer, 2])
+        for head in range(heads):
+            wait_bytes(q_all.at[layer, head, pl.ds(0, n_sp - 1)], q_sems[0].at[layer, head])
+            wait_bytes(num_recv.at[layer, head, pl.ds(0, n_sp - 1)], n_sems[0].at[layer, head])
+        for part in range(parts):
+            wait_bytes(shares.at[layer, part, pl.ds(0, n_tp - 1)], s_sems[0].at[layer, part])
     final.wait()
 
 
@@ -318,7 +336,7 @@
         rows = target.shape[0]
         src_rows = source.shape[0]
         heads = width // HEAD_DIM
-        pad = -(-rows // SUBLANES) * SUBLANES
+        pad = (rows // SUBLANES + 1) * SUBLANES
         anywhere = pl.BlockSpec(memory_space=pl.ANY)
         return pl.pallas_call(
             functools.partial(kernel, n_sp, n_tp),
@@ -340,14 +358,14 @@
                 pltpu.VMEM((layers, src_rows, model), BF16),
                 pltpu.VMEM((layers, heads, src_rows, HEAD_DIM), BF16),
                 pltpu.VMEM((layers, heads, src_rows, HEAD_DIM), BF16),
-                pltpu.VMEM((layers, n_sp, pad, width), BF16),
-                pltpu.VMEM((layers, n_sp, pad, width + LANES), BF16),
-                pltpu.VMEM((layers, n_sp, pad, width + LANES), BF16),
-                pltpu.VMEM((layers, n_tp, pad, model), BF16),
+                pltpu.VMEM((layers, heads, n_sp, pad, HEAD_DIM), BF16),
+                pltpu.VMEM((layers, heads, n_sp, pad, HEAD_DIM), BF16),
+                pltpu.VMEM((layers, heads, n_sp, pad, HEAD_DIM), BF16),
+                pltpu.VMEM((layers, PARTS, n_tp, pad, model // PARTS), BF16),
                 pltpu.SemaphoreType.DMA((6,)),
                 pltpu.SemaphoreType.DMA((layers, 4)),
-                pltpu.SemaphoreType.DMA((layers, 3)),
-                pltpu.SemaphoreType.DMA((layers, 3)),
+                *[pltpu.SemaphoreType.DMA((layers, heads))] * 4,
+                *[pltpu.SemaphoreType.DMA((layers, PARTS))] * 2,
             ],
             compiler_params=pltpu.CompilerParams(
                 collective_id=0, has_side_effects=True, vmem_limit_bytes=60 * 1024 * 1024

time: 33.6 us -> 33.4 us (level)
  no operation moved by 1% of the time
where the time goes in v3:
time: 33.4 us; the launch traced here: 33.2 us
  Pallas kernels  31.8 us (95%)
  local copies, waits for them, and re-layouts  1.38 us (4%)
    pallas_call x1, Pallas kernels, body(): pl.pallas_call(functools.partial(kernel, n_sp, n_tp), out_shape=jax.Shape...  31.8 us
    unnamed x1, local copies, waits for them, and re-layouts  1.38 us

profile of v3, /device:TPU:0, one launch (start us, length us, event | category | flops | bytes accessed | tf_op | source)
XLA Modules:
  0.0 33.2 jit_solution(144989024148016380)
XLA Ops:
  0.0 31.8 %shard_map.91 = bf16[7,2048]{1,0:T(8,128)(2,1)} custom-call(bf16[7,2048]{1,0:T(8,128)(2,1)} %target.1, bf16[256,2048]{1,0:T(8,128)(2,1)} %source.1, f32[2,2048]{1,0:T(2,128)} %tgt_gain.1, f32[2,2048]{1,0:T(2,128)} %src_gain.1, bf16[2,2048,512]{2,1,0:T(8,128)(2,1)} %w_query.1, bf16[2,2048,512]{2,1,0:T(8,128)(2,1)} %w_key.1, bf16[2,2048,512]{2,1,0:T(8,128)(2,1)} %w_value.1, ...), custom_call_target="tpu_custom_call" | custom-call | tf_op jit(solution)/shard_map/pallas_call | solution.py:341
  31.8 1.4 %copy.11 = bf16[7,2048]{1,0:T(8,128)(2,1)} copy(bf16[7,2048]{1,0:T(8,128)(2,1)} %shard_map.91) | data formatting | bytes 57344

commit v4 on v3

--- a/solution.py
+++ b/solution.py
@@ -10,7 +10,7 @@
 
 HEAD_DIM = 256
 EPS = 1e-06
-PARTS = 4
+PARTS = 2
 SUBLANES = 8
 MESH = pl.DeviceIdType.MESH
 BF16 = jnp.bfloat16
@@ -46,7 +46,8 @@
     w_value,
     w_out,
     score_scale,
-    out,
+    out_hid,
+    out_shares,
     tgt_v,
     src_v,
     tg_v,
@@ -56,7 +57,6 @@
     wv_v,
     wo_v,
     scale_s,
-    out_v,
     hid,
     normed,
     keys,
@@ -66,6 +66,7 @@
     num_recv,
     shares,
     load_sem,
+    keep_sem,
     w_sem,
     *sems,
 ):
@@ -115,12 +116,6 @@
             big[layer, kind] = pltpu.make_async_copy(
                 hbm.at[layer], vmem.at[layer], w_sem.at[layer, kind]
             )
-    for copy in small:
-        copy.start()
-    big[0, 0].start()
-    big[0, 1].start()
-    big[0, 2].start()
-
     barrier = pltpu.get_barrier_semaphore()
 
     def greet_sp(step):
@@ -135,6 +130,14 @@
 
     each(n_sp - 1, greet_sp)
     each(n_tp - 1, greet_tp)
+
+    for index in (0, 1):
+        small[index].start()
+    big[0, 0].start()
+    for index in (4, 2, 3):
+        small[index].start()
+    big[0, 1].start()
+    big[0, 2].start()
 
     def remote(src, dst, sems, at, target_id):
         return pltpu.make_async_remote_copy(
@@ -154,19 +157,18 @@
 
     def make_queries(layer):
         hidden = hid[...]
-        normed_tgt = (hidden * row_scale(hidden) * tg_v[layer : layer + 1, :]).astype(BF16)
+        scale = row_scale(hidden)
+        gained = (hidden * tg_v[layer : layer + 1, :]).astype(BF16)
         for head in range(heads):
             cols = slice(head * HEAD_DIM, (head + 1) * HEAD_DIM)
-            block = jnp.dot(normed_tgt, wq_v[layer, :, cols], preferred_element_type=F32)
-            q_all[layer, head, me_s] = head_norm(block)
-            if layer > 0:
-                send_queries(layer, head)
-
-    def send_queries(layer, head):
-        mine = q_all.at[layer, head, me_s]
+            block = jnp.dot(gained, wq_v[layer, :, cols], preferred_element_type=F32)
+            q_all[layer, me_s, head] = head_norm(block * scale)
+
+    def send_queries(layer):
+        mine = q_all.at[layer, me_s]
 
         def go(step):
-            remote(mine, mine, q_sems, (layer, head), {"sp": sp_peer(step)}).start()
+            remote(mine, mine, q_sems, layer, {"sp": sp_peer(step)}).start()
 
         each(n_sp - 1, go)
 
@@ -186,52 +188,55 @@
     chunk = math.gcd(n_sp, 8)
     count = chunk * pad
 
-    def attend(layer, head):
+    def attend(layer):
         def one(step):
             first = step * chunk
-            queries = q_all[layer, head, pl.ds(first, chunk)].astype(F32)
-            scores = lax.dot_general(
-                queries.reshape(count, HEAD_DIM).astype(BF16),
-                keys[layer, head],
-                (((1,), (1,)), ((), ())),
-                preferred_element_type=F32,
-            )
-            weights = jnp.exp(scale_s[layer, head] * (scores / root - root))
-            denom = jnp.sum(weights, axis=1, keepdims=True)
-            numer = jnp.dot(weights.astype(BF16), vals[layer, head], preferred_element_type=F32)
-            high = denom.astype(BF16).astype(F32).reshape(chunk, pad, 1)
-            low = denom.reshape(chunk, pad, 1) - high
             lane = lax.broadcasted_iota(jnp.int32, (chunk, pad, HEAD_DIM), 2)
             row = lax.broadcasted_iota(jnp.int32, (chunk, pad, HEAD_DIM), 1)
-            spread = jnp.where(lane == row, high, jnp.where(lane == row + pad, low, 0.0))
-            packed = jnp.sum(spread, axis=1, keepdims=True)
-            block = jnp.where(row == rows, packed, numer.reshape(chunk, pad, HEAD_DIM))
-            num_send[layer, head, pl.ds(first, chunk)] = block.astype(BF16)
+            for head in range(heads):
+                queries = q_all[layer, pl.ds(first, chunk), head].astype(F32)
+                scores = lax.dot_general(
+                    queries.reshape(count, HEAD_DIM).astype(BF16),
+                    keys[layer, head],
+                    (((1,), (1,)), ((), ())),
+                    preferred_element_type=F32,
+                )
+                weights = jnp.exp(scale_s[layer, head] * (scores / root - root))
+                denom = jnp.sum(weights, axis=1, keepdims=True)
+                numer = jnp.dot(
+                    weights.astype(BF16), vals[layer, head], preferred_element_type=F32
+                )
+                high = denom.astype(BF16).astype(F32).reshape(chunk, pad, 1)
+                low = denom.reshape(chunk, pad, 1) - high
+                spread = jnp.where(lane == row, high, jnp.where(lane == row + pad, low, 0.0))
+                packed = jnp.sum(spread, axis=1, keepdims=True)
+                block = jnp.where(row == rows, packed, numer.reshape(chunk, pad, HEAD_DIM))
+                num_send[layer, pl.ds(first, chunk), head] = block.astype(BF16)
 
         each(n_sp // chunk, one)
 
-    def send_numerators(layer, head):
+    def send_numerators(layer):
         def go(step):
             peer = sp_peer(step)
             remote(
-                num_send.at[layer, head, peer],
-                num_recv.at[layer, head, me_s],
+                num_send.at[layer, peer],
+                num_recv.at[layer, me_s],
                 n_sems,
-                (layer, head),
+                layer,
                 {"sp": peer},
             ).start()
 
         each(n_sp - 1, go)
-        num_recv[layer, head, me_s] = num_send[layer, head, me_s]
+        num_recv[layer, me_s] = num_send[layer, me_s]
 
     def finish_attention(layer):
         pieces = []
         lane = lax.broadcasted_iota(jnp.int32, (pad, HEAD_DIM), 1)
         row = lax.broadcasted_iota(jnp.int32, (pad, HEAD_DIM), 0)
         mine = (lane == row) | (lane == row + pad)
+        wait_bytes(num_recv.at[layer, pl.ds(0, n_sp - 1)], n_sems[1].at[layer])
         for head in range(heads):
-            wait_bytes(num_recv.at[layer, head, pl.ds(0, n_sp - 1)], n_sems[1].at[layer, head])
-            total = jnp.sum(num_recv[layer, head].astype(F32), axis=0)
+            total = jnp.sum(num_recv[layer, :, head].astype(F32), axis=0)
             packed = jnp.broadcast_to(total[rows : rows + 1, :], total.shape)
             denom = jnp.sum(jnp.where(mine, packed, 0.0), axis=1, keepdims=True)
             pieces.append((total / denom).astype(BF16))
@@ -243,11 +248,14 @@
             share = jnp.dot(attended, wo_v[layer, :, cols], preferred_element_type=F32)
             shares[layer, part, me_t] = share.astype(BF16)
             mine = shares.at[layer, part, me_t]
-
-            def go(step, mine=mine, part=part):
-                remote(mine, mine, s_sems, (layer, part), {"tp": tp_peer(step)}).start()
+            there = mine if layer + 1 < layers else out_shares.at[me_t, :, cols]
+
+            def go(step, mine=mine, there=there, part=part):
+                remote(mine, there, s_sems, (layer, part), {"tp": tp_peer(step)}).start()
 
             each(n_tp - 1, go)
+            if layer + 1 == layers:
+                pltpu.make_async_copy(mine, there, keep_sem.at[part]).start()
 
     def add_branch(layer):
         for part in range(parts):
@@ -268,8 +276,7 @@
             if (layer, kind) not in ((0, 0), (0, 1), (0, 2)):
                 big[layer, kind].start()
     pl.semaphore_wait(barrier, n_sp - 1 + n_tp - 1)
-    for head in range(heads):
-        send_queries(0, head)
+    send_queries(0)
 
     small[2].wait()
     small[4].wait()
@@ -293,27 +300,35 @@
         if layer > 0:
             big[layer, 0].wait()
             make_queries(layer)
-        for head in range(heads):
-            wait_bytes(q_all.at[layer, head, pl.ds(0, n_sp - 1)], q_sems[1].at[layer, head])
-            attend(layer, head)
-            send_numerators(layer, head)
+            send_queries(layer)
+        if layer + 1 == layers:
+            tgt_v[...] = hid[0:rows, :].astype(BF16)
+            keep_hidden = pltpu.make_async_copy(tgt_v, out_hid, load_sem.at[0])
+            keep_hidden.start()
+        wait_bytes(q_all.at[layer, pl.ds(0, n_sp - 1)], q_sems[1].at[layer])
+        attend(layer)
+        send_numerators(layer)
         if layer + 1 < layers:
             norm_source(layer + 1)
             make_source(layer + 1)
         big[layer, 3].wait()
         send_shares(layer, finish_attention(layer))
-        add_branch(layer)
-
-    out_v[...] = hid[0:rows, :].astype(BF16)
-    final = pltpu.make_async_copy(out_v, out, load_sem.at[5])
-    final.start()
+        if layer + 1 < layers:
+            add_branch(layer)
+
+    for part in range(parts):
+        cols = slice(part * part_width, (part + 1) * part_width)
+        arrived = out_shares.at[pl.ds(0, n_tp - 1), :, cols]
+        wait_bytes(arrived, s_sems[1].at[layers - 1, part])
+        pltpu.make_async_copy(
+            shares.at[layers - 1, part, me_t], out_shares.at[me_t, :, cols], keep_sem.at[part]
+        ).wait()
+    keep_hidden.wait()
     for layer in range(layers):
-        for head in range(heads):
-            wait_bytes(q_all.at[layer, head, pl.ds(0, n_sp - 1)], q_sems[0].at[layer, head])
-            wait_bytes(num_recv.at[layer, head, pl.ds(0, n_sp - 1)], n_sems[0].at[layer, head])
+        wait_bytes(q_all.at[layer, pl.ds(0, n_sp - 1)], q_sems[0].at[layer])
+        wait_bytes(num_recv.at[layer, pl.ds(0, n_sp - 1)], n_sems[0].at[layer])
         for part in range(parts):
             wait_bytes(shares.at[layer, part, pl.ds(0, n_tp - 1)], s_sems[0].at[layer, part])
-    final.wait()
 
 
 def solution(mesh):
@@ -337,12 +352,15 @@
         src_rows = source.shape[0]
         heads = width // HEAD_DIM
         pad = (rows // SUBLANES + 1) * SUBLANES
-        anywhere = pl.BlockSpec(memory_space=pl.ANY)
-        return pl.pallas_call(
+        anywhere = pl.BlockSpec(memory_space=pltpu.HBM)
+        hidden, last_shares = pl.pallas_call(
             functools.partial(kernel, n_sp, n_tp),
-            out_shape=jax.ShapeDtypeStruct(target.shape, BF16),
+            out_shape=(
+                jax.ShapeDtypeStruct(target.shape, BF16),
+                jax.ShapeDtypeStruct((n_tp, pad, model), BF16),
+            ),
             in_specs=[anywhere] * len(args),
-            out_specs=anywhere,
+            out_specs=(anywhere, anywhere),
             scratch_shapes=[
                 pltpu.VMEM(target.shape, BF16),
                 pltpu.VMEM(source.shape, BF16),
@@ -353,24 +371,28 @@
                 pltpu.VMEM(w_value.shape, BF16),
                 pltpu.VMEM(w_out.shape, BF16),
                 pltpu.SMEM(score_scale.shape, F32),
-                pltpu.VMEM(target.shape, BF16),
                 pltpu.VMEM((pad, model), F32),
                 pltpu.VMEM((layers, src_rows, model), BF16),
                 pltpu.VMEM((layers, heads, src_rows, HEAD_DIM), BF16),
                 pltpu.VMEM((layers, heads, src_rows, HEAD_DIM), BF16),
-                pltpu.VMEM((layers, heads, n_sp, pad, HEAD_DIM), BF16),
-                pltpu.VMEM((layers, heads, n_sp, pad, HEAD_DIM), BF16),
-                pltpu.VMEM((layers, heads, n_sp, pad, HEAD_DIM), BF16),
+                pltpu.VMEM((layers, n_sp, heads, pad, HEAD_DIM), BF16),
+                pltpu.VMEM((layers, n_sp, heads, pad, HEAD_DIM), BF16),
+                pltpu.VMEM((layers, n_sp, heads, pad, HEAD_DIM), BF16),
                 pltpu.VMEM((layers, PARTS, n_tp, pad, model // PARTS), BF16),
-                pltpu.SemaphoreType.DMA((6,)),
+                pltpu.SemaphoreType.DMA((5,)),
+                pltpu.SemaphoreType.DMA((PARTS,)),
                 pltpu.SemaphoreType.DMA((layers, 4)),
-                *[pltpu.SemaphoreType.DMA((layers, heads))] * 4,
+                *[pltpu.SemaphoreType.DMA((layers,))] * 4,
                 *[pltpu.SemaphoreType.DMA((layers, PARTS))] * 2,
             ],
             compiler_params=pltpu.CompilerParams(
                 collective_id=0, has_side_effects=True, vmem_limit_bytes=60 * 1024 * 1024
             ),
         )(*args)
+        branch = last_shares[0, :rows].astype(F32)
+        for group in range(1, n_tp):
+            branch = branch + last_shares[group, :rows].astype(F32)
+        return (hidden.astype(F32) + branch).astype(BF16)
 
     return jax.shard_map(
         body, mesh=mesh, in_specs=placed, out_specs=P("sp", None), check_vma=False

time: 33.4 us -> 32.6 us (0.976)
  other arithmetic: 0 us -> 1.46 us
  local copies, waits for them, and re-layouts: 1.38 us -> 0 us
  Pallas kernels: 31.8 us -> 30.9 us
    convert_element_type x0 -> x1, other arithmetic: none -> 1.46 us  [body(): return (hidden.astype(F32) + branch).astype(BF16)]
    unnamed x1 -> x0, local copies, waits for them, and re-layouts: 1.38 us -> none
    pallas_call x1, Pallas kernels: 31.8 us -> 30.9 us  [body(): pl.pallas_call(functools.partial(kernel, n_sp, n_tp), out_shape=(jax.Shap...]
where the time goes in v4:
time: 32.6 us; the launch traced here: 32.4 us
  Pallas kernels  30.9 us (95%)
  other arithmetic  1.46 us (4%)
    pallas_call x1, Pallas kernels, body(): pl.pallas_call(functools.partial(kernel, n_sp, n_tp), out_shape=(jax.Shap...  30.9 us
    convert_element_type x1, other arithmetic, body(): return (hidden.astype(F32) + branch).astype(BF16)  1.46 us

profile of v4, /device:TPU:0, one launch (start us, length us, event | category | flops | bytes accessed | tf_op | source)
XLA Modules:
  0.0 32.4 jit_solution(11967910504493826741)
XLA Ops:
  0.0 30.9 %shard_map.91 = (bf16[7,2048]{1,0:T(8,128)(2,1)}, bf16[4,8,2048]{2,1,0:T(8,128)(2,1)}) custom-call(bf16[7,2048]{1,0:T(8,128)(2,1)} %target.1, bf16[256,2048]{1,0:T(8,128)(2,1)} %source.1, f32[2,2048]{1,0:T(2,128)} %tgt_gain.1, f32[2,2048]{1,0:T(2,128)} %src_gain.1, bf16[2,2048,512]{2,1,0:T(8,128)(2,1)} %w_query.1, bf16[2,2048,512]{2,1,0:T(8,128)(2,1)} %w_key.1, ...), custom_call_target="tpu_custom_call" | custom-call | tf_op jit(solution)/shard_map/pallas_call | solution.py:356
  30.9 1.5 %fusion = bf16[7,2048]{1,0:T(8,128)(2,1)} fusion(bf16[7,2048]{1,0:T(8,128)(2,1)} %get-tuple-element.7, bf16[4,8,2048]{2,1,0:T(8,128)(2,1)} %get-tuple-element.8), kind=kLoop, calls=%fused_computation.1 | loop fusion | flops 143360 | bytes 172032 | tf_op jit(solution)/shard_map/convert_element_type | solution.py:395
